TPU v7x, 32 devices: a whole 2x2x4 slice. The times are simulated.
32 devices in a mesh: fs: 8 (over z, x), tp: 4 (over y, core).
Axes of the slice: x: 2, y: 2, z: 4, core: 2. Of those that a mesh axis runs over, the one named last changes fastest.
Arguments:
- later_in: bfloat16 [8192, 2048], P('fs'), may hold values from -3 to 3
- earlier_in: bfloat16 [8192, 2048], P('fs'), may hold values from -3 to 3
- cotangent: bfloat16 [8192, 2048], P('fs'), may hold values from -6 to 6
- gate_weight: bfloat16 [2048, 5632], P('fs', 'tp'), may hold values from -0.125 to 0.125
- up_weight: bfloat16 [2048, 5632], P('fs', 'tp'), may hold values from -0.125 to 0.125
- down_weight: bfloat16 [2048, 5632], P('fs', 'tp'), may hold values from -0.078125 to 0.078125
- norm_gain: bfloat16 [2048], replicated, may hold values from 0.099609375 to 1.8984375
- gate_sum: float32 [2048, 5632], P('fs', 'tp'), may hold values from -96 to 96
- up_sum: float32 [2048, 5632], P('fs', 'tp'), may hold values from -96 to 96
- down_sum: float32 [2048, 5632], P('fs', 'tp'), may hold values from -96 to 96
- gain_sum: float32 [2048], replicated, may hold values from -192 to 192
Outputs:
- later_out: bfloat16 [8192, 2048], P(('fs', 'tp'))
- later_hidden: bfloat16 [8192, 5632], P('fs', 'tp')
- earlier_grad: bfloat16 [8192, 2048], P(('fs', 'tp'))
- gate_sum_new: float32 [2048, 5632], P('fs', 'tp')
- up_sum_new: float32 [2048, 5632], P('fs', 'tp')
- down_sum_new: float32 [2048, 5632], P('fs', 'tp')
- gain_sum_new: float32 [2048], replicated
All inputs are finite; a program needn't handle non-finite values.
Results may differ from a plain program's by a relative error of at most 0.013.
Values may be sent and summed in bfloat16 or wider, within the bound.
No kernel may reach another device: no remote copies, remote signals or barrier semaphores. Data moves between devices by JAX's collectives and lax.ppermute only.
A program may use at most 128 MiB of HBM per device.

v0:
```python
import jax
import jax.numpy as jnp
from jax import lax
from jax.sharding import PartitionSpec as P

norm_floor = 0.05


def normalize(tokens_in, norm_gain):
    values = tokens_in.astype(jnp.float32)
    row_scale = lax.rsqrt(jnp.mean(values * values, axis=1, keepdims=True) + norm_floor)
    unit_rows = values * row_scale
    normed = (unit_rows * norm_gain.astype(jnp.float32)).astype(jnp.bfloat16)
    return (row_scale, unit_rows, normed)


def transposed(matrix_a, matrix_b):
    return lax.dot_general(
        matrix_a, matrix_b, (((1,), (1,)), ((), ())), preferred_element_type=jnp.float32
    )


def outer_sum(matrix_a, matrix_b):
    return lax.dot_general(
        matrix_a, matrix_b, (((0,), (0,)), ((), ())), preferred_element_type=jnp.float32
    )


def own_rows(tokens_in, own_count):
    return lax.dynamic_slice_in_dim(tokens_in, lax.axis_index("tp") * own_count, own_count, 0)


def forward(later_in, norm_gain, weights):
    w_gate, w_up, w_down = weights
    normed = normalize(later_in, norm_gain)[2]
    gate_pre = jnp.dot(normed, w_gate, preferred_element_type=jnp.float32)
    up_pre = jnp.dot(normed, w_up, preferred_element_type=jnp.float32)
    hidden = (jax.nn.silu(gate_pre) * up_pre).astype(jnp.bfloat16)
    own_count = later_in.shape[0] // lax.axis_size("tp")
    summed = lax.psum_scatter(
        transposed(hidden, w_down).astype(jnp.bfloat16), "tp", scatter_dimension=0, tiled=True
    ).astype(jnp.float32)
    later_out = (own_rows(later_in, own_count).astype(jnp.float32) + 0.5 * summed).astype(
        jnp.bfloat16
    )
    return (later_out, hidden)


def backward(earlier_in, cotangent, norm_gain, weights):
    w_gate, w_up, w_down = weights
    row_scale, unit_rows, normed = normalize(earlier_in, norm_gain)
    gate_pre = jnp.dot(normed, w_gate, preferred_element_type=jnp.float32)
    up_pre = jnp.dot(normed, w_up, preferred_element_type=jnp.float32)
    sigmoid_gate = jax.nn.sigmoid(gate_pre)
    activated = gate_pre * sigmoid_gate
    hidden = (activated * up_pre).astype(jnp.bfloat16)
    col_width = hidden.shape[1]
    dhidden = jnp.dot(cotangent, w_down, preferred_element_type=jnp.float32)
    dgate = (
        0.5 * dhidden * up_pre * sigmoid_gate * (1.0 + gate_pre * (1.0 - sigmoid_gate))
    ).astype(jnp.bfloat16)
    dupper = (0.5 * dhidden * activated).astype(jnp.bfloat16)
    gate_and_up = jnp.concatenate([dgate, dupper], axis=1)
    dnormed = transposed(dgate, w_gate) + transposed(dupper, w_up)
    gain_part = jnp.sum(dnormed * unit_rows, axis=0)
    weighted = dnormed * norm_gain.astype(jnp.float32)
    branch = row_scale * (
        weighted - unit_rows * jnp.mean(weighted * unit_rows, axis=1, keepdims=True)
    )
    own_count = earlier_in.shape[0] // lax.axis_size("tp")
    summed = lax.psum_scatter(
        branch.astype(jnp.bfloat16), "tp", scatter_dimension=0, tiled=True
    ).astype(jnp.float32)
    earlier_grad = (own_rows(cotangent, own_count).astype(jnp.float32) + summed).astype(
        jnp.bfloat16
    )
    grads_total = lax.psum_scatter(
        jnp.concatenate(
            [outer_sum(normed, gate_and_up), 0.5 * outer_sum(cotangent, hidden)], axis=1
        ).astype(jnp.bfloat16),
        "fs",
        scatter_dimension=0,
        tiled=True,
    ).astype(jnp.float32)
    grad_gate = grads_total[:, :col_width]
    grad_up = grads_total[:, col_width : 2 * col_width]
    grad_down = grads_total[:, 2 * col_width :]
    gain_total = lax.psum(gain_part, ("fs", "tp"))
    return (earlier_grad, grad_gate, grad_up, grad_down, gain_total)


def local(
    later_in,
    earlier_in,
    cotangent,
    gate_weight,
    up_weight,
    down_weight,
    norm_gain,
    gate_sum,
    up_sum,
    down_sum,
    gain_sum,
):
    pieces = (gate_weight, up_weight, down_weight)
    later_out, later_hidden = forward(
        later_in,
        norm_gain,
        (
            lax.all_gather(pieces[0], "fs", axis=0, tiled=True),
            lax.all_gather(pieces[1], "fs", axis=0, tiled=True),
            lax.all_gather(pieces[2], "fs", axis=0, tiled=True),
        ),
    )
    earlier = backward(
        earlier_in,
        cotangent,
        norm_gain,
        (
            lax.all_gather(pieces[0], "fs", axis=0, tiled=True),
            lax.all_gather(pieces[1], "fs", axis=0, tiled=True),
            lax.all_gather(pieces[2], "fs", axis=0, tiled=True),
        ),
    )
    earlier_grad, grad_gate, grad_up, grad_down, gain_total = earlier
    return (
        later_out,
        later_hidden,
        earlier_grad,
        gate_sum + grad_gate,
        up_sum + grad_up,
        down_sum + grad_down,
        gain_sum + gain_total,
    )


def solution(mesh):
    placed = (
        P("fs", None),
        P("fs", None),
        P("fs", None),
        P("fs", "tp"),
        P("fs", "tp"),
        P("fs", "tp"),
        P(),
        P("fs", "tp"),
        P("fs", "tp"),
        P("fs", "tp"),
        P(),
    )
    return jax.shard_map(
        local,
        mesh=mesh,
        in_specs=placed,
        out_specs=(
            P(("fs", "tp"), None),
            P("fs", "tp"),
            P(("fs", "tp"), None),
            P("fs", "tp"),
            P("fs", "tp"),
            P("fs", "tp"),
            P(),
        ),
        check_vma=False,
    )
```

profile of v0, /device:TPU:0, one launch (start us, length us, event | category | flops | bytes accessed | tf_op | source)
XLA Modules:
  0.0 708.4 jit_solution(3213249192349217438)
XLA Ops:
  7.2 0.7 all-gather.4.cloned.1.call-update
  7.9 0.7 all-gather.6.cloned.1.call-update
  8.7 0.0 all-gather.8.cloned.1.call-start
  8.7 0.7 all-gather.8.cloned.1.call-update
  9.4 0.0 reduce-scatter.4.cloned.1.call-start
  9.4 0.8 convert_element_type.59
  10.3 3.3 fusion.4
  13.6 0.9 fusion.13
  14.5 90.8 %all-gather.4.cloned.1.call-done = bf16[2048,1408]{1,0:T(8,128)(2,1)} async-done(((bf16[256,1408]{1,0:T(8,128)(2,1)}), bf16[2048,1408]{1,0:T(8,128)(2,1)}) %all-gather.4.cloned.1.call-update) | async-done | bytes 5767184 | tf_op jit(solution)/shard_map/all_gather | solution.py:110
  105.2 12.0 %fusion.20 = f32[1024,1408]{1,0:T(8,128)} fusion(bf16[2048,1408]{1,0:T(8,128)(2,1)} %all-gather.4.cloned.1.call-done, bf16[1024,2048]{1,0:T(8,128)(2,1)} %param.11, f32[2048]{0:T(1024)S(1)} %convert_element_type.59, f32[1024]{0:T(1024)S(1)} %add_rsqrt_fusion.1), kind=kOutput, calls=%fused_computation.38 | convolution fusion | flops 5913968640 | bytes 15740928 | tf_op jit(solution)/shard_map/dot_general | solution.py:36
  117.2 80.8 %all-gather.6.cloned.1.call-done = bf16[2048,1408]{1,0:T(8,128)(2,1)} async-done(((bf16[256,1408]{1,0:T(8,128)(2,1)}), bf16[2048,1408]{1,0:T(8,128)(2,1)}) %all-gather.6.cloned.1.call-update) | async-done | bytes 5767184 | tf_op jit(solution)/shard_map/all_gather | solution.py:111
  197.9 11.3 %multiply_convert_fusion.4 = bf16[1024,1408]{1,0:T(8,128)(2,1)S(1)} fusion(f32[1024,1408]{1,0:T(8,128)} %fusion.20, bf16[2048,1408]{1,0:T(8,128)(2,1)} %all-gather.6.cloned.1.call-done, bf16[1024,2048]{1,0:T(8,128)(2,1)} %param.11, f32[2048]{0:T(1024)S(1)} %convert_element_type.59, f32[1024]{0:T(1024)S(1)} %add_rsqrt_fusion.1), kind=kOutput, calls=%fused_computation.30 | convolution fusion | flops 5922619392 | bytes 18624512 | tf_op jit(solution)/shard_map/dot_general | solution.py:37
  209.3 81.4 %all-gather.8.cloned.1.call-done = bf16[2048,1408]{1,0:T(8,128)(2,1)} async-done(((bf16[256,1408]{1,0:T(8,128)(2,1)}), bf16[2048,1408]{1,0:T(8,128)(2,1)}) %all-gather.8.cloned.1.call-update) | async-done | bytes 5767184 | tf_op jit(solution)/shard_map/all_gather | solution.py:112
  290.6 10.9 %convolution_convert_fusion.1 = bf16[1024,2048]{1,0:T(8,128)(2,1)} fusion(bf16[1024,1408]{1,0:T(8,128)(2,1)S(1)} %multiply_convert_fusion.4, bf16[2048,1408]{1,0:T(8,128)(2,1)} %all-gather.8.cloned.1.call-done), kind=kOutput, calls=%fused_computation.32 | convolution fusion | flops 5907677184 | bytes 12845056 | tf_op jit(solution)/shard_map/dot_general | solution.py:18
  301.5 0.2 reduce-scatter.6.cloned.1.call-start
  301.8 12.1 %fusion.26 = f32[1024,1408]{1,0:T(8,128)} fusion(bf16[2048,1408]{1,0:T(8,128)(2,1)} %all-gather.4.cloned.1.call-done, bf16[1024,2048]{1,0:T(8,128)(2,1)} %param.12, f32[1024]{0:T(1024)S(1)} %add_rsqrt_fusion, f32[2048]{0:T(1024)S(1)} %convert_element_type.59), kind=kOutput, calls=%fused_computation.44 | convolution fusion | flops 5913968640 | bytes 15740928 | tf_op jit(solution)/shard_map/dot_general | solution.py:52
  313.9 10.7 %fusion.28 = f32[1024,1408]{1,0:T(8,128)} fusion(bf16[2048,1408]{1,0:T(8,128)(2,1)} %all-gather.6.cloned.1.call-done, bf16[1024,2048]{1,0:T(8,128)(2,1)S(1)} %copy-done.1, f32[1024]{0:T(1024)S(1)} %add_rsqrt_fusion, f32[2048]{0:T(1024)S(1)} %convert_element_type.59), kind=kOutput, calls=%fused_computation.45 | convolution fusion | flops 5913968640 | bytes 15740928 | tf_op jit(solution)/shard_map/dot_general | solution.py:53
  324.7 12.3 %multiply_convert_fusion.2 = (bf16[1024,1408]{1,0:T(8,128)(2,1)S(1)}, bf16[1024,1408]{1,0:T(8,128)(2,1)}) fusion(f32[1024,1408]{1,0:T(8,128)} %fusion.26, f32[1024,1408]{1,0:T(8,128)} %fusion.28, bf16[1024,2048]{1,0:T(8,128)(2,1)S(1)} %copy-done.6, bf16[2048,1408]{1,0:T(8,128)(2,1)S(1)} %bitcast.18), kind=kOutput, calls=%fused_computation.26 | convolution fusion | flops 5925765120 | bytes 27262976 | tf_op jit(solution)/shard_map/dot_general | solution.py:58
  337.0 10.2 %fusion.30 = f32[1024,2048]{1,0:T(8,128)} fusion(bf16[1024,1408]{1,0:T(8,128)(2,1)} %get-tuple-element.10, bf16[2048,1408]{1,0:T(8,128)(2,1)S(1)} %bitcast.16), kind=kOutput, calls=%fused_computation.46 | convolution fusion | flops 5905580032 | bytes 17039360 | tf_op jit(solution)/shard_map/dot_general | solution.py:18
  347.2 11.1 %fusion.12 = (f32[2048]{0:T(1024)S(1)}, f32[1024]{0:T(1024)S(1)}, f32[1024,2048]{1,0:T(8,128)S(1)}) fusion(bf16[1024,2048]{1,0:T(8,128)(2,1)S(1)} %copy-done.1, f32[1024]{0:T(1024)S(1)} %add_rsqrt_fusion, f32[2048]{0:T(1024)S(1)} %convert_element_type.59, f32[1024,2048]{1,0:T(8,128)} %fusion.30, bf16[1024,1408]{1,0:T(8,128)(2,1)S(1)} %get-tuple-element.9, ...), kind=kOutput, calls=%fused_computation.19 | convolution fusion | flops 5922354176 | bytes 29646848 | tf_op jit(solution)/shard_map/dot_general | solution.py:18
  358.3 3.5 fusion.11
  361.9 0.0 reduce-scatter.8.cloned.1.call-start
  361.9 13.0 %fusion.14 = bf16[2048,1408]{1,0:T(8,128)(2,1)S(1)} fusion(bf16[1024,2048]{1,0:T(8,128)(2,1)} %param.13, f32[1024,1408]{1,0:T(8,128)} %fusion.28, f32[1024,1408]{1,0:T(8,128)} %fusion.26), kind=kOutput, calls=%fused_computation.21 | convolution fusion | flops 5919997952 | bytes 21495808 | tf_op jit(solution)/shard_map/dot_general | solution.py:24
  374.9 17.4 %convolution_convert_fusion = bf16[2048,2816]{1,0:T(8,128)(2,1)} fusion(bf16[1024,1408]{1,0:T(8,128)(2,1)S(1)} %get-tuple-element.9, bf16[1024,1408]{1,0:T(8,128)(2,1)} %get-tuple-element.10, bf16[1024,2048]{1,0:T(8,128)(2,1)S(1)} %copy-done.2, f32[1024]{0:T(1024)S(1)} %add_rsqrt_fusion, f32[2048]{0:T(1024)S(1)} %convert_element_type.59), kind=kOutput, calls=%fused_computation.2 | convolution fusion | flops 11836850176 | bytes 21508096 | tf_op jit(solution)/shard_map/dot_general | solution.py:24
  392.3 11.8 %pad_maximum_fusion = bf16[2048,4224]{1,0:T(8,128)(2,1)} fusion(bf16[2048,1408]{1,0:T(8,128)(2,1)S(1)} %fusion.14, bf16[2048,2816]{1,0:T(8,128)(2,1)} %convolution_convert_fusion), kind=kLoop, calls=%fused_computation | loop fusion | flops 34603008 | bytes 34603008 | tf_op jit(solution)/shard_map/concatenate | solution.py:78
  404.1 41.4 %psum.7 = f32[2048]{0:T(1024)S(1)} all-reduce(f32[2048]{0:T(1024)S(1)} %get-tuple-element.7), channel_id=1, replica_groups=mesh['fs'=8,'tp'=4] {'fs','tp'}, use_global_device_ids=true, to_apply=%region_7.8 | all-reduce | flops 2048 | bytes 16384 | tf_op jit(solution)/shard_map/psum | solution.py:88
  445.5 0.6 add.71
  446.1 3.1 add_convert_fusion.1
  449.2 2.9 add_convert_fusion
  452.2 245.1 %reduce-scatter.8.cloned.1.call-done = bf16[256,4224]{1,0:T(8,128)(2,1)} async-done(((bf16[2048,4224]{1,0:T(8,128)(2,1)}), bf16[256,4224]{1,0:T(8,128)(2,1)}) %reduce-scatter.8.cloned.1.call-update) | async-done | bytes 2162704 | tf_op jit(solution)/shard_map/reduce_scatter | solution.py:77
  697.2 2.0 convert_element_type.74
  699.3 2.3 slice_add_fusion
  (38 shorter events, 0.2 us)
Async XLA Ops:
  7.2 98.1 %all-gather.4.cloned.1.call-start = ((), (), s32[]{:S(2)}) async-start(), calls=%async_computation.3 | async-start | bytes 6488064 | tf_op jit(solution)/shard_map/all_gather | solution.py:110
  7.9 190.0 %all-gather.6.cloned.1.call-start = ((), (), s32[]{:S(2)}) async-start(), calls=%async_computation.4 | async-start | bytes 6488064 | tf_op jit(solution)/shard_map/all_gather | solution.py:111
  8.7 282.0 %all-gather.8.cloned.1.call-start = ((), (), s32[]{:S(2)}) async-start(), calls=%async_computation.5 | async-start | bytes 6488064 | tf_op jit(solution)/shard_map/all_gather | solution.py:112
  9.4 436.8 %reduce-scatter.4.cloned.1.call-start = ((), (), s32[]{:S(2)}) async-start(), calls=%async_computation.6 | async-start | bytes 5242880 | tf_op jit(solution)/shard_map/reduce_scatter | solution.py:40
  9.4 4.1 copy-start
  209.2 92.3 %copy-start.8 = (bf16[1024,1408]{1,0:T(8,128)(2,1)}, bf16[1024,1408]{1,0:T(8,128)(2,1)S(1)}, u32[]{:S(2)}) copy-start(bf16[1024,1408]{1,0:T(8,128)(2,1)S(1)} %multiply_convert_fusion.4) | copy-start | bytes 8650756
  301.5 147.7 %reduce-scatter.6.cloned.1.call-start = ((), (), s32[]{:S(2)}) async-start(), calls=%async_computation.7 | async-start | bytes 5242880 | tf_op jit(solution)/shard_map/reduce_scatter | solution.py:71
  301.8 12.2 %copy-start.1 = (bf16[1024,2048]{1,0:T(8,128)(2,1)S(1)}, bf16[1024,2048]{1,0:T(8,128)(2,1)}, u32[]{:S(2)}) copy-start(bf16[1024,2048]{1,0:T(8,128)(2,1)} %param.12) | copy-start | bytes 12582916
  301.8 22.9 %slice-start.2 = ((s8[5767168]{0:T(1024)(128)(4,1)}), s8[4194304]{0:T(1024)(128)(4,1)S(1)}, s32[]{:S(2)}) async-start(s8[5767168]{0:T(1024)(128)(4,1)} %bitcast.17), calls=%async_computation.11 | async-start | bytes 8388608
  313.9 10.7 %copy-start.6 = (bf16[1024,2048]{1,0:T(8,128)(2,1)S(1)}, bf16[1024,2048]{1,0:T(8,128)(2,1)}, u32[]{:S(2)}) copy-start(bf16[1024,2048]{1,0:T(8,128)(2,1)} %param.13) | copy-start | bytes 12582916
  313.9 10.7 %slice-start.3 = ((s8[5767168]{0:T(1024)(128)(4,1)}), s8[1572864]{0:T(1024)(128)(4,1)S(1)}, s32[]{:S(2)}) async-start(s8[5767168]{0:T(1024)(128)(4,1)} %bitcast.17), calls=%async_computation.12 | async-start | bytes 3145728
  313.9 23.0 %slice-start = ((s8[5767168]{0:T(1024)(128)(4,1)}), s8[4194304]{0:T(1024)(128)(4,1)S(1)}, s32[]{:S(2)}) async-start(s8[5767168]{0:T(1024)(128)(4,1)} %bitcast.15), calls=%async_computation.9 | async-start | bytes 8388608
  324.7 12.3 %slice-start.1 = ((s8[5767168]{0:T(1024)(128)(4,1)}), s8[1572864]{0:T(1024)(128)(4,1)S(1)}, s32[]{:S(2)}) async-start(s8[5767168]{0:T(1024)(128)(4,1)} %bitcast.15), calls=%async_computation.10 | async-start | bytes 3145728
  361.9 335.4 %reduce-scatter.8.cloned.1.call-start = ((), (), s32[]{:S(2)}) async-start(), calls=%async_computation.8 | async-start | bytes 19464192 | tf_op jit(solution)/shard_map/reduce_scatter | solution.py:77
  361.9 13.0 %copy-start.2 = (bf16[1024,2048]{1,0:T(8,128)(2,1)S(1)}, bf16[1024,2048]{1,0:T(8,128)(2,1)}, u32[]{:S(2)}) copy-start(bf16[1024,2048]{1,0:T(8,128)(2,1)} %param.12) | copy-start | bytes 12582916
  404.1 41.5 %copy-start.7 = (f32[2048]{0:T(1024)S(1)}, f32[2048]{0:T(1024)}, u32[]{:S(2)}) copy-start(f32[2048]{0:T(1024)} %param.21) | copy-start | bytes 24580
  446.1 253.1 %copy-start.3 = (f32[256,1408]{1,0:T(8,128)S(1)}, f32[256,1408]{1,0:T(8,128)}, u32[]{:S(2)}) copy-start(f32[256,1408]{1,0:T(8,128)} %param.20) | copy-start | bytes 4325380
  446.1 253.1 %copy-start.4 = (f32[256,1408]{1,0:T(8,128)S(1)}, f32[256,1408]{1,0:T(8,128)}, u32[]{:S(2)}) copy-start(f32[256,1408]{1,0:T(8,128)} %param.19) | copy-start | bytes 4325380
  697.2 2.0 copy-start.5
Sparse Core Ops, SparseCore 0:
  10.2 95.0 all-gather.3
  107.4 90.4 all-gather.5
  200.1 90.4 all-gather.7
  301.6 42.7 reduce-scatter.3
  362.0 42.7 reduce-scatter.5
  408.6 288.6 reduce-scatter.7
where the time goes:
time: 709 us; the launch traced here: 708 us
  waiting for transfers between devices  500 us (71%)
  matrix products  121 us (17%)
  blocking collectives  41.4 us (6%)
  other arithmetic  31.1 us (4%)
  between operations  14.3 us (2%)
    reduce_scatter x1, waiting for transfers between devices, backward(): lax.psum_scatter(jnp.concatenate([outer_sum(normed, gate_and_up), 0.5 * o...  245 us
    all_gather x1, waiting for transfers between devices, local(): lax.all_gather(pieces[0], 'fs', axis=0, tiled=True)  90.8 us
    all_gather x1, waiting for transfers between devices, local(): lax.all_gather(pieces[2], 'fs', axis=0, tiled=True)  81.4 us
    all_gather x1, waiting for transfers between devices, local(): lax.all_gather(pieces[1], 'fs', axis=0, tiled=True)  80.8 us
    psum x1, blocking collectives, backward(): gain_total = lax.psum(gain_part, ('fs', 'tp'))  41.4 us
    dot_general x3, matrix products, transposed(): lax.dot_general(matrix_a, matrix_b, (((1,), (1,)), ((), ())), preferred_e...  32.2 us
    dot_general x2, matrix products, outer_sum(): lax.dot_general(matrix_a, matrix_b, (((0,), (0,)), ((), ())), preferred_e...  30.4 us
  transfers between devices with their start and end apart: 6, of which 4 were waited for; matrix products, arithmetic and copies ran while one was open for 19% of the time, Pallas kernels for 0%

commit v1 on v0

--- a/solution.py
+++ b/solution.py
@@ -4,6 +4,18 @@
 from jax.sharding import PartitionSpec as P
 
 norm_floor = 0.05
+
+
+def doubled_up(x, axis, dim):
+    ways, here = (lax.axis_size(axis), lax.axis_index(axis))
+    grown, reach = (x, 1)
+    while reach < ways:
+        theirs = lax.ppermute(grown, axis, [(d, d ^ reach) for d in range(ways)])
+        mine_first = jnp.concatenate([grown, theirs], axis=dim)
+        theirs_first = jnp.concatenate([theirs, grown], axis=dim)
+        grown = jnp.where(here & reach == 0, mine_first, theirs_first)
+        reach = 2 * reach
+    return grown
 
 
 def normalize(tokens_in, norm_gain):
@@ -109,7 +121,7 @@
         (
             lax.all_gather(pieces[0], "fs", axis=0, tiled=True),
             lax.all_gather(pieces[1], "fs", axis=0, tiled=True),
-            lax.all_gather(pieces[2], "fs", axis=0, tiled=True),
+            doubled_up(pieces[2], "fs", 0),
         ),
     )
     earlier = backward(

time: 709 us -> 797 us (1.12)
  waiting for transfers between devices: 500 us -> 570 us
    ppermute x0 -> x3, waiting for transfers between devices: none -> 112 us  [doubled_up(): theirs = lax.ppermute(grown, axis, [(d, d ^ reach) for d in range(ways)])]
    all_gather x1, waiting for transfers between devices: 90.8 us -> 6.22 us  [local(): lax.all_gather(pieces[0], 'fs', axis=0, tiled=True)]
    all_gather x1, waiting for transfers between devices: 80.8 us -> 161 us  [local(): lax.all_gather(pieces[1], 'fs', axis=0, tiled=True)]
    all_gather x1, waiting for transfers between devices: 81.4 us -> 34.8 us  [local(): lax.all_gather(pieces[2], 'fs', axis=0, tiled=True)]
    reduce_scatter x1, waiting for transfers between devices: 245 us -> 254 us  [backward(): lax.psum_scatter(jnp.concatenate([outer_sum(normed, gate_and_up), 0.5 * o...]
  transfers between devices with their start and end apart: 6 -> 9, of which waited for: 4 -> 7; matrix products, arithmetic and copies ran while one was open for 19% -> 20% of each run, Pallas kernels for 0% -> 0%
where the time goes in v1:
time: 797 us; the launch traced here: 794 us
  waiting for transfers between devices  570 us (72%)
  matrix products  127 us (16%)
  blocking collectives  39.1 us (5%)
  other arithmetic  38.5 us (5%)
  between operations  14.5 us (2%)
    reduce_scatter x1, waiting for transfers between devices, backward(): lax.psum_scatter(jnp.concatenate([outer_sum(normed, gate_and_up), 0.5 * o...  254 us
    all_gather x1, waiting for transfers between devices, local(): lax.all_gather(pieces[1], 'fs', axis=0, tiled=True)  161 us
    ppermute x3, waiting for transfers between devices, doubled_up(): theirs = lax.ppermute(grown, axis, [(d, d ^ reach) for d in range(ways)])  112 us
    psum x1, blocking collectives, backward(): gain_total = lax.psum(gain_part, ('fs', 'tp'))  39.1 us
    dot_general x3, matrix products, transposed(): lax.dot_general(matrix_a, matrix_b, (((1,), (1,)), ((), ())), preferred_e...  35.9 us
    all_gather x1, waiting for transfers between devices, local(): lax.all_gather(pieces[2], 'fs', axis=0, tiled=True)  34.8 us
    dot_general x2, matrix products, outer_sum(): lax.dot_general(matrix_a, matrix_b, (((0,), (0,)), ((), ())), preferred_e...  31.3 us
  transfers between devices with their start and end apart: 9, of which 7 were waited for; matrix products, arithmetic and copies ran while one was open for 20% of the time, Pallas kernels for 0%

profile of v1, /device:TPU:0, one launch (start us, length us, event | category | flops | bytes accessed | tf_op | source)
XLA Modules:
  0.0 794.3 jit_solution(4489853040333638073)
XLA Ops:
  9.4 3.0 collective-permute-start
  12.5 23.3 %collective-permute-done = bf16[256,1408]{1,0:T(8,128)(2,1)S(1)} collective-permute-done((bf16[256,1408]{1,0:T(8,128)(2,1)}, bf16[256,1408]{1,0:T(8,128)(2,1)S(1)}, u32[]{:S(2)}, u32[]{:S(2)}) %collective-permute-start) | collective-permute-done | bytes 720928 | tf_op jit(solution)/shard_map/ppermute | solution.py:13
  35.8 1.8 maximum_select_fusion.5
  37.5 1.5 collective-permute-start.1
  39.0 0.8 convert_element_type.59
  39.8 3.3 fusion.4
  43.1 0.9 fusion.13
  44.0 72.6 %collective-permute-done.1 = bf16[512,1408]{1,0:T(8,128)(2,1)S(1)} collective-permute-done((bf16[512,1408]{1,0:T(8,128)(2,1)S(1)}, bf16[512,1408]{1,0:T(8,128)(2,1)S(1)}, u32[]{:S(2)}, u32[]{:S(2)}) %collective-permute-start.1) | collective-permute-done | bytes 1441824 | tf_op jit(solution)/shard_map/ppermute | solution.py:13
  116.7 5.5 maximum_select_fusion.4
  122.2 0.7 collective-permute-start.2
  122.9 6.2 all-gather.4.cloned.1.call-done
  129.1 12.0 %fusion.28 = f32[1024,1408]{1,0:T(8,128)} fusion(bf16[2048,1408]{1,0:T(8,128)(2,1)} %all-gather.4.cloned.1.call-done, bf16[1024,2048]{1,0:T(8,128)(2,1)} %param.11, f32[2048]{0:T(1024)S(1)} %convert_element_type.59, f32[1024]{0:T(1024)S(1)} %add_rsqrt_fusion.1), kind=kOutput, calls=%fused_computation.48 | convolution fusion | flops 5913968640 | bytes 15740928 | tf_op jit(solution)/shard_map/dot_general | solution.py:48
  141.1 160.8 %all-gather.6.cloned.1.call-done = bf16[2048,1408]{1,0:T(8,128)(2,1)} async-done(((bf16[256,1408]{1,0:T(8,128)(2,1)}), bf16[2048,1408]{1,0:T(8,128)(2,1)}) %all-gather.6.cloned.1.call-update) | async-done | bytes 5767184 | tf_op jit(solution)/shard_map/all_gather | solution.py:123
  301.8 11.3 %multiply_convert_fusion.4 = bf16[1024,1408]{1,0:T(8,128)(2,1)S(1)} fusion(f32[1024,1408]{1,0:T(8,128)} %fusion.28, bf16[2048,1408]{1,0:T(8,128)(2,1)} %all-gather.6.cloned.1.call-done, bf16[1024,2048]{1,0:T(8,128)(2,1)} %param.11, f32[2048]{0:T(1024)S(1)} %convert_element_type.59, f32[1024]{0:T(1024)S(1)} %add_rsqrt_fusion.1), kind=kOutput, calls=%fused_computation.37 | convolution fusion | flops 5922619392 | bytes 18624512 | tf_op jit(solution)/shard_map/dot_general | solution.py:49
  313.1 15.7 %collective-permute-done.2 = bf16[1024,1408]{1,0:T(8,128)(2,1)S(1)} collective-permute-done((bf16[1024,1408]{1,0:T(8,128)(2,1)}, bf16[1024,1408]{1,0:T(8,128)(2,1)S(1)}, u32[]{:S(2)}, u32[]{:S(2)}) %collective-permute-start.2) | collective-permute-done | bytes 2883616 | tf_op jit(solution)/shard_map/ppermute | solution.py:13
  328.8 11.6 %fusion.26 = bf16[1024,2048]{1,0:T(8,128)(2,1)} fusion(bf16[1024,1408]{1,0:T(8,128)(2,1)S(1)} %multiply_convert_fusion.4, bf16[1024,1408]{1,0:T(8,128)(2,1)S(1)} %collective-permute-done.2, bf16[1024,1408]{1,0:T(8,128)(2,1)} %maximum_select_fusion.4, pred[]{:T(512)S(6)} %eq.9), kind=kOutput, calls=%fused_computation.40 | convolution fusion | flops 5933629440 | bytes 12845057 | tf_op jit(solution)/shard_map/dot_general | solution.py:30
  340.5 12.3 %fusion.35 = f32[1024,1408]{1,0:T(8,128)} fusion(bf16[2048,1408]{1,0:T(8,128)(2,1)} %all-gather.4.cloned.1.call-done, bf16[1024,2048]{1,0:T(8,128)(2,1)} %param.12, f32[1024]{0:T(1024)S(1)} %add_rsqrt_fusion, f32[2048]{0:T(1024)S(1)} %convert_element_type.59), kind=kOutput, calls=%fused_computation.55 | convolution fusion | flops 5913968640 | bytes 15740928 | tf_op jit(solution)/shard_map/dot_general | solution.py:64
  352.8 10.4 %fusion.37 = f32[1024,1408]{1,0:T(8,128)} fusion(bf16[2048,1408]{1,0:T(8,128)(2,1)} %all-gather.6.cloned.1.call-done, bf16[1024,2048]{1,0:T(8,128)(2,1)S(1)} %copy-done.1, f32[1024]{0:T(1024)S(1)} %add_rsqrt_fusion, f32[2048]{0:T(1024)S(1)} %convert_element_type.59), kind=kOutput, calls=%fused_computation.56 | convolution fusion | flops 5913968640 | bytes 15740928 | tf_op jit(solution)/shard_map/dot_general | solution.py:65
  363.2 34.8 %all-gather.8.cloned.1.call-done = bf16[2048,1408]{1,0:T(8,128)(2,1)} async-done(((bf16[256,1408]{1,0:T(8,128)(2,1)}), bf16[2048,1408]{1,0:T(8,128)(2,1)}) %all-gather.8.cloned.1.call-update) | async-done | bytes 5767184 | tf_op jit(solution)/shard_map/all_gather | solution.py:134
  398.0 14.1 %multiply_convert_fusion.2 = (bf16[1024,1408]{1,0:T(8,128)(2,1)S(1)}, bf16[1024,1408]{1,0:T(8,128)(2,1)S(1)}) fusion(f32[1024,1408]{1,0:T(8,128)} %fusion.35, f32[1024,1408]{1,0:T(8,128)} %fusion.37, bf16[1024,2048]{1,0:T(8,128)(2,1)} %param.13, bf16[2048,1408]{1,0:T(8,128)(2,1)} %all-gather.8.cloned.1.call-done), kind=kOutput, calls=%fused_computation.33 | convolution fusion | flops 5925765120 | bytes 27262976 | tf_op jit(solution)/shard_map/dot_general | solution.py:70
  412.2 12.8 %fusion.39 = f32[1024,2048]{1,0:T(8,128)} fusion(bf16[1024,1408]{1,0:T(8,128)(2,1)S(1)} %get-tuple-element.10, bf16[2048,1408]{1,0:T(8,128)(2,1)} %all-gather.4.cloned.1.call-done), kind=kOutput, calls=%fused_computation.57 | convolution fusion | flops 5905580032 | bytes 17039360 | tf_op jit(solution)/shard_map/dot_general | solution.py:30
  425.0 11.4 %fusion.12 = (f32[2048]{0:T(1024)S(1)}, f32[1024]{0:T(1024)S(1)}, f32[1024,2048]{1,0:T(8,128)S(1)}) fusion(bf16[1024,2048]{1,0:T(8,128)(2,1)S(1)} %copy-done.2, f32[1024]{0:T(1024)S(1)} %add_rsqrt_fusion, f32[2048]{0:T(1024)S(1)} %convert_element_type.59, f32[1024,2048]{1,0:T(8,128)} %fusion.39, bf16[1024,1408]{1,0:T(8,128)(2,1)S(1)} %get-tuple-element.9, ...), kind=kOutput, calls=%fused_computation.19 | convolution fusion | flops 5922354176 | bytes 29646848 | tf_op jit(solution)/shard_map/dot_general | solution.py:30
  436.4 3.5 fusion.11
  440.0 12.4 %fusion.14 = bf16[2048,1408]{1,0:T(8,128)(2,1)S(1)} fusion(bf16[1024,2048]{1,0:T(8,128)(2,1)} %param.13, f32[1024,1408]{1,0:T(8,128)} %fusion.37, f32[1024,1408]{1,0:T(8,128)} %fusion.35), kind=kOutput, calls=%fused_computation.21 | convolution fusion | flops 5919997952 | bytes 21495808 | tf_op jit(solution)/shard_map/dot_general | solution.py:36
  452.4 18.9 %convolution_convert_fusion = bf16[2048,2816]{1,0:T(8,128)(2,1)} fusion(bf16[1024,1408]{1,0:T(8,128)(2,1)} %copy-done.9, bf16[1024,1408]{1,0:T(8,128)(2,1)} %copy-done.10, bf16[1024,2048]{1,0:T(8,128)(2,1)S(1)} %copy-done.3, f32[1024]{0:T(1024)S(1)} %add_rsqrt_fusion, f32[2048]{0:T(1024)S(1)} %convert_element_type.59), kind=kOutput, calls=%fused_computation.2 | convolution fusion | flops 11836850176 | bytes 21508096 | tf_op jit(solution)/shard_map/dot_general | solution.py:36
  471.3 11.8 %pad_maximum_fusion = bf16[2048,4224]{1,0:T(8,128)(2,1)} fusion(bf16[2048,1408]{1,0:T(8,128)(2,1)S(1)} %fusion.14, bf16[2048,2816]{1,0:T(8,128)(2,1)} %convolution_convert_fusion), kind=kLoop, calls=%fused_computation | loop fusion | flops 34603008 | bytes 34603008 | tf_op jit(solution)/shard_map/concatenate | solution.py:90
  483.1 39.1 %psum.7 = f32[2048]{0:T(1024)S(1)} all-reduce(f32[2048]{0:T(1024)S(1)} %get-tuple-element.7), channel_id=1, replica_groups=mesh['fs'=8,'tp'=4] {'fs','tp'}, use_global_device_ids=true, to_apply=%region_7.8 | all-reduce | flops 2048 | bytes 16384 | tf_op jit(solution)/shard_map/psum | solution.py:100
  522.8 3.1 add_convert_fusion.1
  526.0 3.0 add_convert_fusion
  528.9 254.0 %reduce-scatter.8.cloned.1.call-done = bf16[256,4224]{1,0:T(8,128)(2,1)} async-done(((bf16[2048,4224]{1,0:T(8,128)(2,1)}), bf16[256,4224]{1,0:T(8,128)(2,1)}) %reduce-scatter.8.cloned.1.call-update) | async-done | bytes 2162704 | tf_op jit(solution)/shard_map/reduce_scatter | solution.py:89
  782.9 2.0 convert_element_type.74
  785.0 2.3 slice_add_fusion
  (40 shorter events, 3.0 us)
Async XLA Ops:
  7.2 121.9 %all-gather.4.cloned.1.call-start = ((), (), s32[]{:S(2)}) async-start(), calls=%async_computation.3 | async-start | bytes 6488064 | tf_op jit(solution)/shard_map/all_gather | solution.py:122
  7.9 293.9 %all-gather.6.cloned.1.call-start = ((), (), s32[]{:S(2)}) async-start(), calls=%async_computation.4 | async-start | bytes 6488064 | tf_op jit(solution)/shard_map/all_gather | solution.py:123
  8.7 389.4 %all-gather.8.cloned.1.call-start = ((), (), s32[]{:S(2)}) async-start(), calls=%async_computation.6 | async-start | bytes 6488064 | tf_op jit(solution)/shard_map/all_gather | solution.py:134
  9.4 513.5 %reduce-scatter.4.cloned.1.call-start = ((), (), s32[]{:S(2)}) async-start(), calls=%async_computation.5 | async-start | bytes 5242880 | tf_op jit(solution)/shard_map/reduce_scatter | solution.py:52
  9.4 26.3 %collective-permute-start = (bf16[256,1408]{1,0:T(8,128)(2,1)}, bf16[256,1408]{1,0:T(8,128)(2,1)S(1)}, u32[]{:S(2)}, u32[]{:S(2)}) collective-permute-start(bf16[256,1408]{1,0:T(8,128)(2,1)} %param.16), channel_id=1, source_target_pairs={{0,4},{4,0},{8,12},{12,8},{16,20},{20,16},{24,28},{28,24},{1,5},{5... | collective-permute-start | bytes 2162696 | tf_op jit(solution)/shard_map/ppermute | solution.py:13
  37.5 79.1 %collective-permute-start.1 = (bf16[512,1408]{1,0:T(8,128)(2,1)S(1)}, bf16[512,1408]{1,0:T(8,128)(2,1)S(1)}, u32[]{:S(2)}, u32[]{:S(2)}) collective-permute-start(bf16[512,1408]{1,0:T(8,128)(2,1)S(1)} %maximum_select_fusion.5), channel_id=1, source_target_pairs={{0,8},{4,12},{8,0},{12,4},{16,24},{20,28},{24,16},{28,20},{1,9},{5... | collective-permute-start | bytes 4325384 | tf_op jit(solution)/shard_map/ppermute | solution.py:13
  39.0 4.1 copy-start
  122.2 206.7 %collective-permute-start.2 = (bf16[1024,1408]{1,0:T(8,128)(2,1)}, bf16[1024,1408]{1,0:T(8,128)(2,1)S(1)}, u32[]{:S(2)}, u32[]{:S(2)}) collective-permute-start(bf16[1024,1408]{1,0:T(8,128)(2,1)} %maximum_select_fusion.4), channel_id=1, source_target_pairs={{0,16},{4,20},{8,24},{12,28},{16,0},{20,4},{24,8},{28,12},{1,17},{... | collective-permute-start | bytes 8650760 | tf_op jit(solution)/shard_map/ppermute | solution.py:13
  313.1 15.7 %copy-start.8 = (bf16[1024,1408]{1,0:T(8,128)(2,1)}, bf16[1024,1408]{1,0:T(8,128)(2,1)S(1)}, u32[]{:S(2)}) copy-start(bf16[1024,1408]{1,0:T(8,128)(2,1)S(1)} %multiply_convert_fusion.4) | copy-start | bytes 8650756
  340.5 185.5 %reduce-scatter.6.cloned.1.call-start = ((), (), s32[]{:S(2)}) async-start(), calls=%async_computation.7 | async-start | bytes 5242880 | tf_op jit(solution)/shard_map/reduce_scatter | solution.py:83
  340.5 12.3 %copy-start.1 = (bf16[1024,2048]{1,0:T(8,128)(2,1)S(1)}, bf16[1024,2048]{1,0:T(8,128)(2,1)}, u32[]{:S(2)}) copy-start(bf16[1024,2048]{1,0:T(8,128)(2,1)} %param.12) | copy-start | bytes 12582916
  412.2 12.9 %copy-start.10 = (bf16[1024,1408]{1,0:T(8,128)(2,1)}, bf16[1024,1408]{1,0:T(8,128)(2,1)S(1)}, u32[]{:S(2)}) copy-start(bf16[1024,1408]{1,0:T(8,128)(2,1)S(1)} %get-tuple-element.10) | copy-start | bytes 8650756
  412.2 12.9 %copy-start.9 = (bf16[1024,1408]{1,0:T(8,128)(2,1)}, bf16[1024,1408]{1,0:T(8,128)(2,1)S(1)}, u32[]{:S(2)}) copy-start(bf16[1024,1408]{1,0:T(8,128)(2,1)S(1)} %get-tuple-element.9) | copy-start | bytes 8650756
  412.2 12.9 %copy-start.2 = (bf16[1024,2048]{1,0:T(8,128)(2,1)S(1)}, bf16[1024,2048]{1,0:T(8,128)(2,1)}, u32[]{:S(2)}) copy-start(bf16[1024,2048]{1,0:T(8,128)(2,1)} %param.12) | copy-start | bytes 12582916
  440.0 343.0 %reduce-scatter.8.cloned.1.call-start = ((), (), s32[]{:S(2)}) async-start(), calls=%async_computation.8 | async-start | bytes 19464192 | tf_op jit(solution)/shard_map/reduce_scatter | solution.py:89
  440.0 12.4 %copy-start.3 = (bf16[1024,2048]{1,0:T(8,128)(2,1)S(1)}, bf16[1024,2048]{1,0:T(8,128)(2,1)}, u32[]{:S(2)}) copy-start(bf16[1024,2048]{1,0:T(8,128)(2,1)} %param.12) | copy-start | bytes 12582916
  483.1 39.1 %copy-start.7 = (f32[2048]{0:T(1024)S(1)}, f32[2048]{0:T(1024)}, u32[]{:S(2)}) copy-start(f32[2048]{0:T(1024)} %param.21) | copy-start | bytes 24580
  522.8 262.1 %copy-start.4 = (f32[256,1408]{1,0:T(8,128)S(1)}, f32[256,1408]{1,0:T(8,128)}, u32[]{:S(2)}) copy-start(f32[256,1408]{1,0:T(8,128)} %param.20) | copy-start | bytes 4325380
  522.8 262.1 %copy-start.5 = (f32[256,1408]{1,0:T(8,128)S(1)}, f32[256,1408]{1,0:T(8,128)}, u32[]{:S(2)}) copy-start(f32[256,1408]{1,0:T(8,128)} %param.19) | copy-start | bytes 4325380
  782.9 2.0 copy-start.6
Sparse Core Ops, SparseCore 0:
  10.2 118.8 all-gather.3
  131.3 170.4 all-gather.5
  304.0 94.0 all-gather.7
  400.4 42.7 reduce-scatter.3
  445.6 44.7 reduce-scatter.5
  494.1 288.7 reduce-scatter.7
